TPU v7x, 128 devices: a whole 4x4x4 slice. The times are simulated.
128 devices in a mesh: pp: 4 (over x), fs: 4 (over y), tp: 8 (over z, core).
Axes of the slice: x: 4, y: 4, z: 4, core: 2. Of those that a mesh axis runs over, the one named last changes fastest.
Arguments:
- micro_in: bfloat16 [2, 96, 1024], P(None, 'pp', ('tp', 'fs')), may hold values from -6 to 6
- norm_gain: float32 [4, 1024], P('pp'), may hold values from 0.5 to 1.5
- proj_gate: bfloat16 [4, 1024, 8, 4, 64], P('pp', None, 'tp', 'fs'), may hold values from -0.1875 to 0.1875
- proj_value: bfloat16 [4, 1024, 8, 4, 64], P('pp', None, 'tp', 'fs'), may hold values from -0.1875 to 0.1875
- proj_write: bfloat16 [4, 1024, 8, 128], P('pp', None, 'tp'), may hold values from -0.1875 to 0.1875
- proj_read: bfloat16 [4, 1024, 8, 128], P('pp', None, 'tp'), may hold values from -0.1875 to 0.1875
- proj_step: bfloat16 [4, 1024, 2, 8, 4], P('pp', None, None, 'tp', 'fs'), may hold values from -0.1875 to 0.1875
- step_bias: float32 [4, 2, 8, 4], P('pp', None, 'tp', 'fs'), may hold values from -4.6 to -2.3
- decay_log: float32 [4, 2, 8, 4], P('pp', None, 'tp', 'fs'), may hold values from 0 to 2.77
- skip_gain: float32 [4, 8, 4], P('pp', 'tp', 'fs'), may hold values from 0.5 to 1.5
- conv_value: float32 [4, 5, 8, 4, 64], P('pp', None, 'tp', 'fs'), may hold values from -2.5 to 2.5
- conv_write: float32 [4, 5, 8, 128], P('pp', None, 'tp'), may hold values from -2.5 to 2.5
- conv_read: float32 [4, 5, 8, 128], P('pp', None, 'tp'), may hold values from -2.5 to 2.5
- proj_out: bfloat16 [4, 8, 4, 64, 1024], P('pp', 'tp', 'fs'), may hold values from -0.125 to 0.125
Outputs:
- mixed_out: bfloat16 [2, 96, 1024], P(None, 'pp', ('tp', 'fs'))
All inputs are finite; a program needn't handle non-finite values.
Results may differ from a plain program's by a relative error of at most 0.025.
Values may be sent and summed in bfloat16 or wider, within the bound.
No kernel may reach another device: no remote copies, remote signals or barrier semaphores. Data moves between devices by JAX's collectives and lax.ppermute only.
A program may use at most 64 MiB of HBM per device.

v0:
```python
import jax
import jax.numpy as jnp
from jax import lax
from jax.sharding import Mesh
from jax.sharding import PartitionSpec as P

TP_FS = ("tp_0", "tp_1", "fs")
TP = ("tp_0", "tp_1")
epsilon = 1e-06


def sum_in_order(parts, axes, order):
    lengths = [lax.axis_size(a) for a in axes]
    parts = parts.reshape(*lengths, *parts.shape[1:])
    parts = parts.transpose(*order, *range(len(axes), parts.ndim))
    parts = parts.reshape(-1, *parts.shape[len(axes) :])
    for k in order:
        parts = lax.psum_scatter(parts, axes[k], scatter_dimension=0, tiled=True)
    return parts[0]


def cut_along(shard, dim, peers):
    lengths = shard.shape
    parts = shard.reshape(*lengths[:dim], peers, lengths[dim] // peers, *lengths[dim + 1 :])
    return jnp.moveaxis(parts, dim, 0)


def sum_by_axis(shard, axes, order, dim):
    peers = lax.axis_size(axes)
    return sum_in_order(cut_along(shard, dim, peers), axes, order)


def own_rows_2(term, span, axes, order):
    running = term(jnp.int32(0), span * lax.axis_size(axes)).astype(jnp.bfloat16)
    return sum_by_axis(running, axes, order, 0).astype(jnp.float32)


def passed_along(shard, axis, by):
    peers = lax.axis_size(axis)
    pairs = [(i, i + by) for i in range(peers) if 0 <= i + by < peers]
    return lax.ppermute(shard, axis, pairs)


def from_root(shard, axis, root):
    return lax.dynamic_index_in_dim(lax.all_gather(shard, axis), root, 0, keepdims=False)


def total_of_pieces(shard, axis):
    return lax.all_gather(shard, axis).sum(0)


def centred_conv(signal, conv_taps):
    span_width = conv_taps.shape[0]
    half_width = span_width // 2
    length = signal.shape[0]
    padded = jnp.pad(signal, ((half_width, half_width), (0, 0)))
    running = jnp.zeros_like(signal)
    for offset in range(span_width):
        running = running + padded[offset : offset + length] * conv_taps[offset]
    return running


def duality_mix(
    gate_flat,
    value_flat,
    write_flat,
    read_flat,
    step_raw,
    step_bias,
    decay_log,
    skip_gain,
    conv_value,
    conv_write,
    conv_read,
):
    groups, per_group = skip_gain.shape
    length = gate_flat.shape[0]
    head_size = value_flat.shape[1] // (groups * per_group)
    state_size = write_flat.shape[1] // groups
    taps_count = conv_value.shape[0]
    value_act = jax.nn.silu(
        centred_conv(value_flat.astype(jnp.float32), conv_value.reshape(taps_count, -1))
    ).astype(jnp.bfloat16)
    write_act = jax.nn.silu(
        centred_conv(write_flat.astype(jnp.float32), conv_write.reshape(taps_count, -1))
    ).astype(jnp.bfloat16)
    read_act = jax.nn.silu(
        centred_conv(read_flat.astype(jnp.float32), conv_read.reshape(taps_count, -1))
    ).astype(jnp.bfloat16)
    step_size = jax.nn.softplus(step_raw.reshape(length, 2, groups, per_group) + step_bias[None])
    log_decay = step_size * (-jnp.exp(decay_log))[None]
    fwd_cum = jnp.cumsum(log_decay[:, 0], axis=0)
    bwd_cum = jnp.flip(jnp.cumsum(jnp.flip(log_decay[:, 1], 0), axis=0), 0)
    positions = jnp.arange(length)
    lower_mask = (positions[:, None] >= positions[None, :])[:, :, None, None]
    upper_mask = (positions[:, None] <= positions[None, :])[:, :, None, None]
    fwd_weight = (
        jnp.exp(jnp.where(lower_mask, fwd_cum[:, None] - fwd_cum[None, :], -jnp.inf))
        * step_size[None, :, 0]
    )
    bwd_weight = (
        jnp.exp(jnp.where(upper_mask, bwd_cum[:, None] - bwd_cum[None, :], -jnp.inf))
        * step_size[None, :, 1]
    )
    scores = jnp.einsum(
        "tgn,sgn->tsg",
        read_act.reshape(length, groups, state_size),
        write_act.reshape(length, groups, state_size),
        preferred_element_type=jnp.float32,
    )
    combined = scores[:, :, :, None] * (fwd_weight + bwd_weight)
    value_heads = value_act.reshape(length, groups, per_group, head_size).astype(jnp.float32)
    mixed_heads = jnp.einsum(
        "tsgh,sghp->tghp", combined, value_heads, precision=lax.Precision.HIGHEST
    )
    mixed_heads = mixed_heads + skip_gain[None, :, :, None] * value_heads
    return (mixed_heads.reshape(length, -1) * jax.nn.silu(gate_flat.astype(jnp.float32))).astype(
        jnp.bfloat16
    )


def per_device(
    micro_in,
    norm_gain,
    proj_gate,
    proj_value,
    proj_write,
    proj_read,
    proj_step,
    step_bias,
    decay_log,
    skip_gain,
    conv_value,
    conv_write,
    conv_read,
    proj_out,
):
    section_count = lax.axis_size("pp")
    section_idx = lax.axis_index("pp")
    width_model = norm_gain.shape[1]
    fed_blocks = lax.all_gather(micro_in, "pp", axis=1, tiled=True)
    micro_count = fed_blocks.shape[0]
    length = fed_blocks.shape[1]
    fed_columns = jnp.swapaxes(fed_blocks, 1, 2)
    gain_vec = norm_gain[0].astype(jnp.float32)
    cut_gate = proj_gate.shape[2] * proj_gate.shape[3] * proj_gate.shape[4]
    cut_write = proj_write.shape[2] * proj_write.shape[3]
    weight_all = jnp.concatenate(
        [
            proj_gate[0].reshape(width_model, -1),
            proj_value[0].reshape(width_model, -1),
            proj_write[0].reshape(width_model, -1),
            proj_read[0].reshape(width_model, -1),
            proj_step[0].reshape(width_model, -1),
        ],
        axis=1,
    )
    out_weights = proj_out[0].reshape(-1, width_model)
    own_rows = width_model // lax.axis_size(TP_FS)

    def project(column_block):
        gathered = lax.all_gather(column_block, TP_FS, axis=0, tiled=True)
        as_float = gathered.astype(jnp.float32)
        scale_rms = lax.rsqrt(jnp.mean(as_float * as_float, axis=0) + epsilon)
        normed = (as_float * scale_rms[None, :] * gain_vec[:, None]).astype(jnp.bfloat16)
        return lax.dot_general(
            normed, weight_all, (((0,), (0,)), ((), ())), preferred_element_type=jnp.float32
        )

    def term_maker(token_rows):

        def term_rows(offset, span_count):
            weight_cols = lax.dynamic_slice_in_dim(out_weights, offset, span_count, 1)
            return lax.dot_general(
                weight_cols,
                token_rows,
                (((0,), (1,)), ((), ())),
                preferred_element_type=jnp.float32,
            )

        return term_rows

    def mix_block(column_block):
        projected = project(column_block)
        gate_flat = projected[:, :cut_gate].astype(jnp.bfloat16)
        value_flat = projected[:, cut_gate : 2 * cut_gate].astype(jnp.bfloat16)
        write_flat = projected[:, 2 * cut_gate : 2 * cut_gate + cut_write].astype(jnp.bfloat16)
        read_flat = projected[:, 2 * cut_gate + cut_write : 2 * cut_gate + 2 * cut_write].astype(
            jnp.bfloat16
        )
        step_raw = projected[:, 2 * cut_gate + 2 * cut_write :]
        gated_out = duality_mix(
            gate_flat,
            value_flat,
            write_flat,
            read_flat,
            step_raw,
            step_bias[0],
            decay_log[0],
            skip_gain[0],
            conv_value[0],
            conv_write[0],
            conv_read[0],
        )
        summed = own_rows_2(term_maker(gated_out), own_rows, TP_FS, (1, 0, 2))
        branch = lax.optimization_barrier(summed.astype(jnp.bfloat16))
        return (column_block.astype(jnp.float32) + 0.5 * branch.astype(jnp.float32)).astype(
            jnp.bfloat16
        )

    total_steps = micro_count + section_count - 1

    def advance(moment, loop_state):
        arriving, collected = loop_state
        pick_index = jnp.clip(moment, 0, micro_count - 1)
        fresh_block = lax.dynamic_index_in_dim(fed_columns, pick_index, 0, keepdims=False)
        current = jnp.where(section_idx == 0, fresh_block, arriving)
        produced = mix_block(current)
        slot_index = moment - section_idx
        keep_flag = (
            (section_idx == section_count - 1) & (slot_index >= 0) & (slot_index < micro_count)
        )
        slot_safe = jnp.clip(slot_index, 0, micro_count - 1)
        previous = lax.dynamic_index_in_dim(collected, slot_safe, 0, keepdims=False)
        collected = lax.dynamic_update_index_in_dim(
            collected, jnp.where(keep_flag, produced, previous), slot_safe, 0
        )
        arriving = passed_along(produced, "pp", 1)
        return (arriving, collected)

    start_loop = (jnp.zeros_like(fed_columns[0]), jnp.zeros_like(fed_columns))
    arriving, collected = lax.fori_loop(0, total_steps, advance, start_loop)
    shared = from_root(collected, "pp", section_count - 1)
    token_share = length // section_count
    own_block = lax.dynamic_slice_in_dim(shared, section_idx * token_share, token_share, 2)
    as_float = own_block.astype(jnp.float32)
    partial_squares = jnp.sum(as_float * as_float, axis=1)
    total_squares = total_of_pieces(partial_squares, TP_FS)
    scale_rms = lax.rsqrt(total_squares / width_model + epsilon)
    result = (as_float * scale_rms[:, None, :]).astype(jnp.bfloat16)
    return jnp.swapaxes(result, 1, 2)


def solution(mesh):
    split = Mesh(
        mesh.devices.reshape(mesh.shape["pp"], mesh.shape["fs"], 4, 2), ("pp", "fs", "tp_0", "tp_1")
    )
    in_specs = (
        P(None, "pp", TP_FS),
        P("pp", None),
        P("pp", None, TP, "fs", None),
        P("pp", None, TP, "fs", None),
        P("pp", None, TP, None),
        P("pp", None, TP, None),
        P("pp", None, None, TP, "fs"),
        P("pp", None, TP, "fs"),
        P("pp", None, TP, "fs"),
        P("pp", TP, "fs"),
        P("pp", None, TP, "fs", None),
        P("pp", None, TP, None),
        P("pp", None, TP, None),
        P("pp", TP, "fs", None, None),
    )
    out_specs = P(None, "pp", TP_FS)
    return jax.shard_map(
        per_device, mesh=split, in_specs=in_specs, out_specs=out_specs, check_vma=False
    )
```

profile of v0, /device:TPU:1, one launch (start us, length us, event | category | flops | bytes accessed | tf_op | source)
XLA Modules:
  0.0 630.5 jit_solution(568530465908368264)
XLA Ops:
  6.5 1.1 copy.61
  8.7 2.2 concatenate.3
  11.0 10.3 %all_gather.25 = bf16[2,96,32]{2,0,1:T(2,128)(2,1)S(1)} all-gather(bf16[2,24,32]{2,0,1:T(2,128)(2,1)S(1)} %copy.60), channel_id=1, replica_groups=mesh['pp'=4,'fs'=4,'tp_0'=4,'tp_1'=2] {'pp'}, dimensions={1}, use_global_device_ids=true | all-gather | bytes 15360 | tf_op jit(solution)/shard_map/all_gather | solution.py:141
  21.4 0.7 copy-done.11
  22.1 0.6 copy-done.4
  22.8 547.7 %while.17 = (s32[]{:T(128)}, bf16[32,96]{1,0:T(8,128)(2,1)S(1)}, bf16[2,32,96]{2,1,0:T(8,128)(2,1)S(1)}, pred[]{:T(512)}, bf16[2,32,96]{2,1,0:T(8,128)(2,1)S(1)}...) while((s32[]{:T(128)}, bf16[32,96]{1,0:T(8,128)(2,1)S(1)}, ...), condition=%wide.region_7.8_spmd, body=%wide.region_0.7_spmd.sunk | while | flops 99476072 | bytes 4874331 | solution.py:232
  22.8 45.5 %all_gather.31 = bf16[1024,96]{1,0:T(8,128)(2,1)S(1)} all-gather(bf16[32,96]{1,0:T(8,128)(2,1)S(1)} %bitcast_select_fusion.3), channel_id=1, replica_groups=mesh['pp'=4,'fs'=4,'tp_0'=4,'tp_1'=2] {'tp_0','tp_1','fs'}, dimensions={0}, use_global_device_ids=true | all-gather | bytes 202752 | tf_op jit(solution)/shard_map/while/body/eval_jaxpr/all_gather | solution.py:162
  68.4 0.6 fusion.72
  69.6 0.8 reverse_reduce_fusion.2
  71.0 0.9 fusion.75
  72.2 0.7 copy.77
  73.0 10.9 %reduce-scatter.4.cloned.1.call-done = bf16[16,32,96]{2,1,0:T(8,128)(2,1)} async-done(((bf16[32,32,96]{2,1,0:T(8,128)(2,1)}), bf16[16,32,96]{2,1,0:T(8,128)(2,1)}) %reduce-scatter.4.cloned.1.call-update) | async-done | bytes 98320 | tf_op jit(solution)/shard_map/while/body/eval_jaxpr/reduce_scatter | solution.py:18
  84.0 21.8 %reduce-scatter.6.cloned.1.call-done = bf16[4,32,96]{2,1,0:T(8,128)(2,1)} async-done(((bf16[16,32,96]{2,1,0:T(8,128)(2,1)}), bf16[4,32,96]{2,1,0:T(8,128)(2,1)}) %reduce-scatter.6.cloned.1.call-update) | async-done | bytes 24592 | tf_op jit(solution)/shard_map/while/body/eval_jaxpr/reduce_scatter | solution.py:18
  105.8 22.5 %reduce-scatter.8.cloned.1.call-done = bf16[1,32,96]{2,1,0:T(8,128)(2,1)} async-done(((bf16[4,32,96]{2,1,0:T(8,128)(2,1)}), bf16[1,32,96]{2,1,0:T(8,128)(2,1)}) %reduce-scatter.8.cloned.1.call-update) | async-done | bytes 6160 | tf_op jit(solution)/shard_map/while/body/eval_jaxpr/reduce_scatter | solution.py:18
  128.3 0.7 bitcast_dynamic-update-slice_fusion.2
  129.0 3.1 collective-permute-start
  132.2 0.8 collective-permute-done
  132.9 44.5 %all_gather.31 = bf16[1024,96]{1,0:T(8,128)(2,1)S(1)} all-gather(bf16[32,96]{1,0:T(8,128)(2,1)S(1)} %bitcast_select_fusion.3), channel_id=1, replica_groups=mesh['pp'=4,'fs'=4,'tp_0'=4,'tp_1'=2] {'tp_0','tp_1','fs'}, dimensions={0}, use_global_device_ids=true | all-gather | bytes 202752 | tf_op jit(solution)/shard_map/while/body/eval_jaxpr/all_gather | solution.py:162
  177.6 0.6 fusion.72
  178.8 0.8 reverse_reduce_fusion.2
  180.2 0.9 fusion.75
  181.4 0.7 copy.77
  182.2 11.3 %reduce-scatter.4.cloned.1.call-done = bf16[16,32,96]{2,1,0:T(8,128)(2,1)} async-done(((bf16[32,32,96]{2,1,0:T(8,128)(2,1)}), bf16[16,32,96]{2,1,0:T(8,128)(2,1)}) %reduce-scatter.4.cloned.1.call-update) | async-done | bytes 98320 | tf_op jit(solution)/shard_map/while/body/eval_jaxpr/reduce_scatter | solution.py:18
  193.6 21.6 %reduce-scatter.6.cloned.1.call-done = bf16[4,32,96]{2,1,0:T(8,128)(2,1)} async-done(((bf16[16,32,96]{2,1,0:T(8,128)(2,1)}), bf16[4,32,96]{2,1,0:T(8,128)(2,1)}) %reduce-scatter.6.cloned.1.call-update) | async-done | bytes 24592 | tf_op jit(solution)/shard_map/while/body/eval_jaxpr/reduce_scatter | solution.py:18
  215.3 22.3 %reduce-scatter.8.cloned.1.call-done = bf16[1,32,96]{2,1,0:T(8,128)(2,1)} async-done(((bf16[4,32,96]{2,1,0:T(8,128)(2,1)}), bf16[1,32,96]{2,1,0:T(8,128)(2,1)}) %reduce-scatter.8.cloned.1.call-update) | async-done | bytes 6160 | tf_op jit(solution)/shard_map/while/body/eval_jaxpr/reduce_scatter | solution.py:18
  237.6 0.7 bitcast_dynamic-update-slice_fusion.2
  238.3 3.1 collective-permute-start
  241.4 0.8 collective-permute-done
  242.2 44.6 %all_gather.31 = bf16[1024,96]{1,0:T(8,128)(2,1)S(1)} all-gather(bf16[32,96]{1,0:T(8,128)(2,1)S(1)} %bitcast_select_fusion.3), channel_id=1, replica_groups=mesh['pp'=4,'fs'=4,'tp_0'=4,'tp_1'=2] {'tp_0','tp_1','fs'}, dimensions={0}, use_global_device_ids=true | all-gather | bytes 202752 | tf_op jit(solution)/shard_map/while/body/eval_jaxpr/all_gather | solution.py:162
  286.9 0.6 fusion.72
  288.1 0.8 reverse_reduce_fusion.2
  289.5 0.9 fusion.75
  290.7 0.7 copy.77
  291.5 11.3 %reduce-scatter.4.cloned.1.call-done = bf16[16,32,96]{2,1,0:T(8,128)(2,1)} async-done(((bf16[32,32,96]{2,1,0:T(8,128)(2,1)}), bf16[16,32,96]{2,1,0:T(8,128)(2,1)}) %reduce-scatter.4.cloned.1.call-update) | async-done | bytes 98320 | tf_op jit(solution)/shard_map/while/body/eval_jaxpr/reduce_scatter | solution.py:18
  302.9 21.7 %reduce-scatter.6.cloned.1.call-done = bf16[4,32,96]{2,1,0:T(8,128)(2,1)} async-done(((bf16[16,32,96]{2,1,0:T(8,128)(2,1)}), bf16[4,32,96]{2,1,0:T(8,128)(2,1)}) %reduce-scatter.6.cloned.1.call-update) | async-done | bytes 24592 | tf_op jit(solution)/shard_map/while/body/eval_jaxpr/reduce_scatter | solution.py:18
  324.7 22.5 %reduce-scatter.8.cloned.1.call-done = bf16[1,32,96]{2,1,0:T(8,128)(2,1)} async-done(((bf16[4,32,96]{2,1,0:T(8,128)(2,1)}), bf16[1,32,96]{2,1,0:T(8,128)(2,1)}) %reduce-scatter.8.cloned.1.call-update) | async-done | bytes 6160 | tf_op jit(solution)/shard_map/while/body/eval_jaxpr/reduce_scatter | solution.py:18
  347.2 0.7 bitcast_dynamic-update-slice_fusion.2
  347.9 3.1 collective-permute-start
  351.0 0.8 collective-permute-done
  351.8 44.5 %all_gather.31 = bf16[1024,96]{1,0:T(8,128)(2,1)S(1)} all-gather(bf16[32,96]{1,0:T(8,128)(2,1)S(1)} %bitcast_select_fusion.3), channel_id=1, replica_groups=mesh['pp'=4,'fs'=4,'tp_0'=4,'tp_1'=2] {'tp_0','tp_1','fs'}, dimensions={0}, use_global_device_ids=true | all-gather | bytes 202752 | tf_op jit(solution)/shard_map/while/body/eval_jaxpr/all_gather | solution.py:162
  396.4 0.6 fusion.72
  397.6 0.8 reverse_reduce_fusion.2
  399.0 0.9 fusion.75
  400.3 0.7 copy.77
  401.1 11.4 %reduce-scatter.4.cloned.1.call-done = bf16[16,32,96]{2,1,0:T(8,128)(2,1)} async-done(((bf16[32,32,96]{2,1,0:T(8,128)(2,1)}), bf16[16,32,96]{2,1,0:T(8,128)(2,1)}) %reduce-scatter.4.cloned.1.call-update) | async-done | bytes 98320 | tf_op jit(solution)/shard_map/while/body/eval_jaxpr/reduce_scatter | solution.py:18
  412.5 21.7 %reduce-scatter.6.cloned.1.call-done = bf16[4,32,96]{2,1,0:T(8,128)(2,1)} async-done(((bf16[16,32,96]{2,1,0:T(8,128)(2,1)}), bf16[4,32,96]{2,1,0:T(8,128)(2,1)}) %reduce-scatter.6.cloned.1.call-update) | async-done | bytes 24592 | tf_op jit(solution)/shard_map/while/body/eval_jaxpr/reduce_scatter | solution.py:18
  434.3 22.3 %reduce-scatter.8.cloned.1.call-done = bf16[1,32,96]{2,1,0:T(8,128)(2,1)} async-done(((bf16[4,32,96]{2,1,0:T(8,128)(2,1)}), bf16[1,32,96]{2,1,0:T(8,128)(2,1)}) %reduce-scatter.8.cloned.1.call-update) | async-done | bytes 6160 | tf_op jit(solution)/shard_map/while/body/eval_jaxpr/reduce_scatter | solution.py:18
  456.6 0.7 bitcast_dynamic-update-slice_fusion.2
  457.3 3.1 collective-permute-start
  460.4 0.8 collective-permute-done
  461.2 44.6 %all_gather.31 = bf16[1024,96]{1,0:T(8,128)(2,1)S(1)} all-gather(bf16[32,96]{1,0:T(8,128)(2,1)S(1)} %bitcast_select_fusion.3), channel_id=1, replica_groups=mesh['pp'=4,'fs'=4,'tp_0'=4,'tp_1'=2] {'tp_0','tp_1','fs'}, dimensions={0}, use_global_device_ids=true | all-gather | bytes 202752 | tf_op jit(solution)/shard_map/while/body/eval_jaxpr/all_gather | solution.py:162
  505.9 0.6 fusion.72
  507.1 0.8 reverse_reduce_fusion.2
  508.5 0.9 fusion.75
  509.7 0.7 copy.77
  510.5 11.3 %reduce-scatter.4.cloned.1.call-done = bf16[16,32,96]{2,1,0:T(8,128)(2,1)} async-done(((bf16[32,32,96]{2,1,0:T(8,128)(2,1)}), bf16[16,32,96]{2,1,0:T(8,128)(2,1)}) %reduce-scatter.4.cloned.1.call-update) | async-done | bytes 98320 | tf_op jit(solution)/shard_map/while/body/eval_jaxpr/reduce_scatter | solution.py:18
  521.9 21.6 %reduce-scatter.6.cloned.1.call-done = bf16[4,32,96]{2,1,0:T(8,128)(2,1)} async-done(((bf16[16,32,96]{2,1,0:T(8,128)(2,1)}), bf16[4,32,96]{2,1,0:T(8,128)(2,1)}) %reduce-scatter.6.cloned.1.call-update) | async-done | bytes 24592 | tf_op jit(solution)/shard_map/while/body/eval_jaxpr/reduce_scatter | solution.py:18
  543.6 22.3 %reduce-scatter.8.cloned.1.call-done = bf16[1,32,96]{2,1,0:T(8,128)(2,1)} async-done(((bf16[4,32,96]{2,1,0:T(8,128)(2,1)}), bf16[1,32,96]{2,1,0:T(8,128)(2,1)}) %reduce-scatter.8.cloned.1.call-update) | async-done | bytes 6160 | tf_op jit(solution)/shard_map/while/body/eval_jaxpr/reduce_scatter | solution.py:18
  565.9 0.7 bitcast_dynamic-update-slice_fusion.2
  566.6 3.1 collective-permute-start
  569.7 0.8 collective-permute-done
  570.5 10.1 %all-gather = bf16[8,32,96]{2,1,0:T(8,128)(2,1)S(1)} all-gather(bf16[2,32,96]{2,1,0:T(8,128)(2,1)S(1)} %get-tuple-element.349), channel_id=2, replica_groups=mesh['pp'=4,'fs'=4,'tp_0'=4,'tp_1'=2] {'pp'}, dimensions={0}, use_global_device_ids=true | all-gather | bytes 61440 | tf_op jit(solution)/shard_map/all_gather | solution.py:45
  580.7 42.5 %all-gather.2 = f32[32,2,24]{2,1,0:T(2,128)S(1)} all-gather(f32[1,2,24]{2,1,0:T(2,128)S(1)} %bitcast.173), channel_id=3, replica_groups=mesh['pp'=4,'fs'=4,'tp_0'=4,'tp_1'=2] {'tp_0','tp_1','fs'}, dimensions={0}, use_global_device_ids=true | all-gather | bytes 6336 | tf_op jit(solution)/shard_map/all_gather | solution.py:49
  623.3 0.7 copy.65
  (174 shorter events, 10.4 us)
Async XLA Ops:
  6.5 1.1 copy-start.3
  6.5 1.3 copy-start.10
  7.7 1.0 copy-start.1
  7.7 1.0 copy-start.2
  8.7 2.2 copy-start.9
  10.9 11.2 %copy-start = (bf16[1,1,1,64,1024]{4,3,2,1,0:T(8,128)(2,1)S(1)}, bf16[1,1,1,64,1024]{4,3,2,1,0:T(8,128)(2,1)}, u32[]{:S(2)}) copy-start(bf16[1,1,1,64,1024]{4,3,2,1,0:T(8,128)(2,1)} %param.29) | copy-start | bytes 393220
  21.3 0.8 copy-start.6
  21.3 0.8 copy-start.7
  21.4 0.7 copy-start.11
  22.0 0.7 copy-start.4
  22.1 0.7 copy-start.5
  22.1 0.7 copy-start.8
  22.8 61.2 %reduce-scatter.4.cloned.1.call-start = ((), (), s32[]{:S(2)}) async-start(), calls=%async_computation.3 | async-start | bytes 393216 | tf_op jit(solution)/shard_map/while/body/eval_jaxpr/reduce_scatter | solution.py:18
  73.0 32.8 %reduce-scatter.6.cloned.1.call-start = ((), (), s32[]{:S(2)}) async-start(), calls=%async_computation.4 | async-start | bytes 163840 | tf_op jit(solution)/shard_map/while/body/eval_jaxpr/reduce_scatter | solution.py:18
  84.0 44.4 %reduce-scatter.8.cloned.1.call-start = ((), (), s32[]{:S(2)}) async-start(), calls=%async_computation.5 | async-start | bytes 40960 | tf_op jit(solution)/shard_map/while/body/eval_jaxpr/reduce_scatter | solution.py:18
  129.0 3.9 collective-permute-start
  132.9 60.6 %reduce-scatter.4.cloned.1.call-start = ((), (), s32[]{:S(2)}) async-start(), calls=%async_computation.3 | async-start | bytes 393216 | tf_op jit(solution)/shard_map/while/body/eval_jaxpr/reduce_scatter | solution.py:18
  182.2 33.0 %reduce-scatter.6.cloned.1.call-start = ((), (), s32[]{:S(2)}) async-start(), calls=%async_computation.4 | async-start | bytes 163840 | tf_op jit(solution)/shard_map/while/body/eval_jaxpr/reduce_scatter | solution.py:18
  193.6 44.0 %reduce-scatter.8.cloned.1.call-start = ((), (), s32[]{:S(2)}) async-start(), calls=%async_computation.5 | async-start | bytes 40960 | tf_op jit(solution)/shard_map/while/body/eval_jaxpr/reduce_scatter | solution.py:18
  238.3 3.9 collective-permute-start
  242.2 60.7 %reduce-scatter.4.cloned.1.call-start = ((), (), s32[]{:S(2)}) async-start(), calls=%async_computation.3 | async-start | bytes 393216 | tf_op jit(solution)/shard_map/while/body/eval_jaxpr/reduce_scatter | solution.py:18
  291.5 33.2 %reduce-scatter.6.cloned.1.call-start = ((), (), s32[]{:S(2)}) async-start(), calls=%async_computation.4 | async-start | bytes 163840 | tf_op jit(solution)/shard_map/while/body/eval_jaxpr/reduce_scatter | solution.py:18
  302.9 44.3 %reduce-scatter.8.cloned.1.call-start = ((), (), s32[]{:S(2)}) async-start(), calls=%async_computation.5 | async-start | bytes 40960 | tf_op jit(solution)/shard_map/while/body/eval_jaxpr/reduce_scatter | solution.py:18
  347.9 3.9 collective-permute-start
  351.7 60.7 %reduce-scatter.4.cloned.1.call-start = ((), (), s32[]{:S(2)}) async-start(), calls=%async_computation.3 | async-start | bytes 393216 | tf_op jit(solution)/shard_map/while/body/eval_jaxpr/reduce_scatter | solution.py:18
  401.0 33.2 %reduce-scatter.6.cloned.1.call-start = ((), (), s32[]{:S(2)}) async-start(), calls=%async_computation.4 | async-start | bytes 163840 | tf_op jit(solution)/shard_map/while/body/eval_jaxpr/reduce_scatter | solution.py:18
  412.5 44.2 %reduce-scatter.8.cloned.1.call-start = ((), (), s32[]{:S(2)}) async-start(), calls=%async_computation.5 | async-start | bytes 40960 | tf_op jit(solution)/shard_map/while/body/eval_jaxpr/reduce_scatter | solution.py:18
  457.3 3.8 collective-permute-start
  461.2 60.7 %reduce-scatter.4.cloned.1.call-start = ((), (), s32[]{:S(2)}) async-start(), calls=%async_computation.3 | async-start | bytes 393216 | tf_op jit(solution)/shard_map/while/body/eval_jaxpr/reduce_scatter | solution.py:18
  510.5 33.1 %reduce-scatter.6.cloned.1.call-start = ((), (), s32[]{:S(2)}) async-start(), calls=%async_computation.4 | async-start | bytes 163840 | tf_op jit(solution)/shard_map/while/body/eval_jaxpr/reduce_scatter | solution.py:18
  521.9 44.0 %reduce-scatter.8.cloned.1.call-start = ((), (), s32[]{:S(2)}) async-start(), calls=%async_computation.5 | async-start | bytes 40960 | tf_op jit(solution)/shard_map/while/body/eval_jaxpr/reduce_scatter | solution.py:18
  566.6 3.9 collective-permute-start
Sparse Core Ops, SparseCore 0:
  73.1 10.8 reduce-scatter.3
  86.3 19.4 reduce-scatter.5
  108.1 20.1 reduce-scatter.7
  182.3 11.2 reduce-scatter.3
  195.8 19.4 reduce-scatter.5
  217.4 20.0 reduce-scatter.7
  291.6 11.2 reduce-scatter.3
  305.2 19.4 reduce-scatter.5
  327.0 20.1 reduce-scatter.7
  401.1 11.2 reduce-scatter.3
  414.8 19.4 reduce-scatter.5
  436.4 20.1 reduce-scatter.7
  510.6 11.2 reduce-scatter.3
  524.1 19.4 reduce-scatter.5
  545.7 20.1 reduce-scatter.7
where the time goes:
time: 631 us; the launch traced here: 630 us
  blocking collectives  287 us (45%)
  waiting for transfers between devices  281 us (45%)
  local copies, waits for them, and re-layouts  16.9 us (3%)
  starting transfers between devices  15.9 us (3%)
  between operations  13.2 us (2%)
  matrix products  9.24 us (1%)
  other arithmetic  7.19 us (1%)
    reduce_scatter x15, waiting for transfers between devices, sum_in_order(): parts = lax.psum_scatter(parts, axes[k], scatter_dimension=0, tiled=True)  277 us
    all_gather x5, blocking collectives, project(): gathered = lax.all_gather(column_block, TP_FS, axis=0, tiled=True)  224 us
    all_gather x1, blocking collectives, total_of_pieces(): return lax.all_gather(shard, axis).sum(0)  42.5 us
    ppermute x5, starting transfers between devices, passed_along(): return lax.ppermute(shard, axis, pairs)  15.4 us
  transfers between devices with their start and end apart: 20, of which 20 were waited for; matrix products, arithmetic and copies ran while one was open for 0% of the time, Pallas kernels for 0%

commit v1 on v0

--- a/solution.py
+++ b/solution.py
@@ -159,7 +159,9 @@
     own_rows = width_model // lax.axis_size(TP_FS)
 
     def project(column_block):
-        gathered = lax.all_gather(column_block, TP_FS, axis=0, tiled=True)
+        gathered = jnp.concatenate(
+            lax.all_to_all(jnp.stack([column_block] * lax.axis_size(TP_FS)), TP_FS, 0, 0), axis=0
+        )
         as_float = gathered.astype(jnp.float32)
         scale_rms = lax.rsqrt(jnp.mean(as_float * as_float, axis=0) + epsilon)
         normed = (as_float * scale_rms[None, :] * gain_vec[:, None]).astype(jnp.bfloat16)

time: 631 us -> 494 us (0.78)
  blocking collectives: 287 us -> 62.8 us
  starting transfers between devices: 15.9 us -> 65 us
  waiting for transfers between devices: 281 us -> 314 us
    all_gather x5 -> x0, blocking collectives: 224 us -> none  [project(): gathered = lax.all_gather(column_block, TP_FS, axis=0, tiled=True)]
    all_to_all x0 -> x5, starting transfers between devices: none -> 48.9 us  [project(): lax.all_to_all(jnp.stack([column_block] * lax.axis_size(TP_FS)), TP_FS, 0...]
    all_to_all x0 -> x5, waiting for transfers between devices: none -> 44 us  [project(): lax.all_to_all(jnp.stack([column_block] * lax.axis_size(TP_FS)), TP_FS, 0...]
    reduce_scatter x15, waiting for transfers between devices: 277 us -> 266 us  [sum_in_order(): parts = lax.psum_scatter(parts, axes[k], scatter_dimension=0, tiled=True)]
  transfers between devices with their start and end apart: 20 -> 25, of which waited for: 20 -> 25; matrix products, arithmetic and copies ran while one was open for 0% -> 0% of each run, Pallas kernels for 0% -> 0%
where the time goes in v1:
time: 494 us; the launch traced here: 493 us
  waiting for transfers between devices  314 us (64%)
  starting transfers between devices  65 us (13%)
  blocking collectives  62.8 us (13%)
  local copies, waits for them, and re-layouts  20.6 us (4%)
  between operations  13.2 us (3%)
  other arithmetic  8.23 us (2%)
  matrix products  8.09 us (2%)
    reduce_scatter x15, waiting for transfers between devices, sum_in_order(): parts = lax.psum_scatter(parts, axes[k], scatter_dimension=0, tiled=True)  266 us
    all_to_all x5, starting transfers between devices, project(): lax.all_to_all(jnp.stack([column_block] * lax.axis_size(TP_FS)), TP_FS, 0...  48.9 us
    all_to_all x5, waiting for transfers between devices, project(): lax.all_to_all(jnp.stack([column_block] * lax.axis_size(TP_FS)), TP_FS, 0...  44 us
    all_gather x1, blocking collectives, total_of_pieces(): return lax.all_gather(shard, axis).sum(0)  42.5 us
    ppermute x5, starting transfers between devices, passed_along(): return lax.ppermute(shard, axis, pairs)  15.5 us
    all_gather x1, blocking collectives, per_device(): fed_blocks = lax.all_gather(micro_in, 'pp', axis=1, tiled=True)  10.3 us
    all_gather x1, blocking collectives, from_root(): lax.all_gather(shard, axis)  10 us
  transfers between devices with their start and end apart: 25, of which 25 were waited for; matrix products, arithmetic and copies ran while one was open for 0% of the time, Pallas kernels for 0%

profile of v1, /device:TPU:1, one launch (start us, length us, event | category | flops | bytes accessed | tf_op | source)
XLA Modules:
  0.0 493.3 jit_solution(6209931284737676635)
XLA Ops:
  6.5 1.1 copy.72
  8.7 2.2 concatenate.3
  11.0 10.3 %all_gather.15 = bf16[2,96,32]{2,0,1:T(2,128)(2,1)S(1)} all-gather(bf16[2,24,32]{2,0,1:T(2,128)(2,1)S(1)} %copy.71), channel_id=1, replica_groups=mesh['pp'=4,'fs'=4,'tp_0'=4,'tp_1'=2] {'pp'}, dimensions={1}, use_global_device_ids=true | all-gather | bytes 15360 | tf_op jit(solution)/shard_map/all_gather | solution.py:141
  22.8 410.6 %while.17 = (s32[]{:T(128)}, bf16[32,96]{1,0:T(8,128)(2,1)S(1)}, bf16[2,32,96]{2,1,0:T(8,128)(2,1)S(1)}, pred[]{:T(512)}, bf16[2,32,96]{2,1,0:T(8,128)(2,1)S(1)}...) while((s32[]{:T(128)}, bf16[32,96]{1,0:T(8,128)(2,1)S(1)}, ...), condition=%wide.region_7.8_spmd, body=%wide.region_0.7_spmd.sunk | while | flops 99476072 | bytes 5988475 | solution.py:234
  22.8 0.7 stack.7
  23.5 11.7 %all-to-all-start = ((bf16[32,32,96]{2,1,0:T(8,128)(2,1)}), bf16[32,32,96]{2,1,0:T(8,128)(2,1)S(1)}, u32[]{:S(2)}, u32[]{:S(2)}) async-start(bf16[32,32,96]{2,1,0:T(8,128)(2,1)} %stack.7), calls=%async_computation | async-start | bytes 524288 | tf_op jit(solution)/shard_map/while/body/eval_jaxpr/all_to_all | solution.py:163
  35.2 8.8 %all-to-all-done = bf16[32,32,96]{2,1,0:T(8,128)(2,1)S(1)} async-done(((bf16[32,32,96]{2,1,0:T(8,128)(2,1)}), bf16[32,32,96]{2,1,0:T(8,128)(2,1)S(1)}, u32[]{:S(2)}, u32[]{:S(2)}) %all-to-all-start) | async-done | bytes 196640 | tf_op jit(solution)/shard_map/while/body/eval_jaxpr/all_to_all | solution.py:163
  45.3 0.8 reverse_reduce_fusion.2
  46.7 0.9 fusion.73
  48.0 0.7 copy.88
  48.8 8.1 %reduce-scatter.4.cloned.1.call-done = bf16[16,32,96]{2,1,0:T(8,128)(2,1)} async-done(((bf16[32,32,96]{2,1,0:T(8,128)(2,1)}), bf16[16,32,96]{2,1,0:T(8,128)(2,1)}) %reduce-scatter.4.cloned.1.call-update) | async-done | bytes 98320 | tf_op jit(solution)/shard_map/while/body/eval_jaxpr/reduce_scatter | solution.py:18
  56.9 21.7 %reduce-scatter.6.cloned.1.call-done = bf16[4,32,96]{2,1,0:T(8,128)(2,1)} async-done(((bf16[16,32,96]{2,1,0:T(8,128)(2,1)}), bf16[4,32,96]{2,1,0:T(8,128)(2,1)}) %reduce-scatter.6.cloned.1.call-update) | async-done | bytes 24592 | tf_op jit(solution)/shard_map/while/body/eval_jaxpr/reduce_scatter | solution.py:18
  78.7 22.5 %reduce-scatter.8.cloned.1.call-done = bf16[1,32,96]{2,1,0:T(8,128)(2,1)} async-done(((bf16[4,32,96]{2,1,0:T(8,128)(2,1)}), bf16[1,32,96]{2,1,0:T(8,128)(2,1)}) %reduce-scatter.8.cloned.1.call-update) | async-done | bytes 6160 | tf_op jit(solution)/shard_map/while/body/eval_jaxpr/reduce_scatter | solution.py:18
  101.2 0.7 bitcast_dynamic-update-slice_fusion.2
  101.9 3.1 collective-permute-start
  105.1 0.8 collective-permute-done
  105.8 0.7 stack.7
  106.6 9.3 %all-to-all-start = ((bf16[32,32,96]{2,1,0:T(8,128)(2,1)}), bf16[32,32,96]{2,1,0:T(8,128)(2,1)S(1)}, u32[]{:S(2)}, u32[]{:S(2)}) async-start(bf16[32,32,96]{2,1,0:T(8,128)(2,1)} %stack.7), calls=%async_computation | async-start | bytes 524288 | tf_op jit(solution)/shard_map/while/body/eval_jaxpr/all_to_all | solution.py:163
  116.0 8.8 %all-to-all-done = bf16[32,32,96]{2,1,0:T(8,128)(2,1)S(1)} async-done(((bf16[32,32,96]{2,1,0:T(8,128)(2,1)}), bf16[32,32,96]{2,1,0:T(8,128)(2,1)S(1)}, u32[]{:S(2)}, u32[]{:S(2)}) %all-to-all-start) | async-done | bytes 196640 | tf_op jit(solution)/shard_map/while/body/eval_jaxpr/all_to_all | solution.py:163
  126.1 0.8 reverse_reduce_fusion.2
  127.4 0.9 fusion.73
  128.7 0.7 copy.88
  129.5 9.5 %reduce-scatter.4.cloned.1.call-done = bf16[16,32,96]{2,1,0:T(8,128)(2,1)} async-done(((bf16[32,32,96]{2,1,0:T(8,128)(2,1)}), bf16[16,32,96]{2,1,0:T(8,128)(2,1)}) %reduce-scatter.4.cloned.1.call-update) | async-done | bytes 98320 | tf_op jit(solution)/shard_map/while/body/eval_jaxpr/reduce_scatter | solution.py:18
  139.0 21.6 %reduce-scatter.6.cloned.1.call-done = bf16[4,32,96]{2,1,0:T(8,128)(2,1)} async-done(((bf16[16,32,96]{2,1,0:T(8,128)(2,1)}), bf16[4,32,96]{2,1,0:T(8,128)(2,1)}) %reduce-scatter.6.cloned.1.call-update) | async-done | bytes 24592 | tf_op jit(solution)/shard_map/while/body/eval_jaxpr/reduce_scatter | solution.py:18
  160.7 22.3 %reduce-scatter.8.cloned.1.call-done = bf16[1,32,96]{2,1,0:T(8,128)(2,1)} async-done(((bf16[4,32,96]{2,1,0:T(8,128)(2,1)}), bf16[1,32,96]{2,1,0:T(8,128)(2,1)}) %reduce-scatter.8.cloned.1.call-update) | async-done | bytes 6160 | tf_op jit(solution)/shard_map/while/body/eval_jaxpr/reduce_scatter | solution.py:18
  183.0 0.7 bitcast_dynamic-update-slice_fusion.2
  183.7 3.1 collective-permute-start
  186.8 0.8 collective-permute-done
  187.6 0.7 stack.7
  188.3 9.3 %all-to-all-start = ((bf16[32,32,96]{2,1,0:T(8,128)(2,1)}), bf16[32,32,96]{2,1,0:T(8,128)(2,1)S(1)}, u32[]{:S(2)}, u32[]{:S(2)}) async-start(bf16[32,32,96]{2,1,0:T(8,128)(2,1)} %stack.7), calls=%async_computation | async-start | bytes 524288 | tf_op jit(solution)/shard_map/while/body/eval_jaxpr/all_to_all | solution.py:163
  197.7 8.8 %all-to-all-done = bf16[32,32,96]{2,1,0:T(8,128)(2,1)S(1)} async-done(((bf16[32,32,96]{2,1,0:T(8,128)(2,1)}), bf16[32,32,96]{2,1,0:T(8,128)(2,1)S(1)}, u32[]{:S(2)}, u32[]{:S(2)}) %all-to-all-start) | async-done | bytes 196640 | tf_op jit(solution)/shard_map/while/body/eval_jaxpr/all_to_all | solution.py:163
  207.8 0.8 reverse_reduce_fusion.2
  209.2 0.9 fusion.73
  210.4 0.7 copy.88
  211.2 9.5 %reduce-scatter.4.cloned.1.call-done = bf16[16,32,96]{2,1,0:T(8,128)(2,1)} async-done(((bf16[32,32,96]{2,1,0:T(8,128)(2,1)}), bf16[16,32,96]{2,1,0:T(8,128)(2,1)}) %reduce-scatter.4.cloned.1.call-update) | async-done | bytes 98320 | tf_op jit(solution)/shard_map/while/body/eval_jaxpr/reduce_scatter | solution.py:18
  220.8 21.8 %reduce-scatter.6.cloned.1.call-done = bf16[4,32,96]{2,1,0:T(8,128)(2,1)} async-done(((bf16[16,32,96]{2,1,0:T(8,128)(2,1)}), bf16[4,32,96]{2,1,0:T(8,128)(2,1)}) %reduce-scatter.6.cloned.1.call-update) | async-done | bytes 24592 | tf_op jit(solution)/shard_map/while/body/eval_jaxpr/reduce_scatter | solution.py:18
  242.6 22.5 %reduce-scatter.8.cloned.1.call-done = bf16[1,32,96]{2,1,0:T(8,128)(2,1)} async-done(((bf16[4,32,96]{2,1,0:T(8,128)(2,1)}), bf16[1,32,96]{2,1,0:T(8,128)(2,1)}) %reduce-scatter.8.cloned.1.call-update) | async-done | bytes 6160 | tf_op jit(solution)/shard_map/while/body/eval_jaxpr/reduce_scatter | solution.py:18
  265.8 3.1 collective-permute-start
  268.9 0.8 collective-permute-done
  269.7 0.7 stack.7
  270.4 9.3 %all-to-all-start = ((bf16[32,32,96]{2,1,0:T(8,128)(2,1)}), bf16[32,32,96]{2,1,0:T(8,128)(2,1)S(1)}, u32[]{:S(2)}, u32[]{:S(2)}) async-start(bf16[32,32,96]{2,1,0:T(8,128)(2,1)} %stack.7), calls=%async_computation | async-start | bytes 524288 | tf_op jit(solution)/shard_map/while/body/eval_jaxpr/all_to_all | solution.py:163
  279.8 8.8 %all-to-all-done = bf16[32,32,96]{2,1,0:T(8,128)(2,1)S(1)} async-done(((bf16[32,32,96]{2,1,0:T(8,128)(2,1)}), bf16[32,32,96]{2,1,0:T(8,128)(2,1)S(1)}, u32[]{:S(2)}, u32[]{:S(2)}) %all-to-all-start) | async-done | bytes 196640 | tf_op jit(solution)/shard_map/while/body/eval_jaxpr/all_to_all | solution.py:163
  289.9 0.8 reverse_reduce_fusion.2
  291.3 0.9 fusion.73
  292.5 0.7 copy.88
  293.3 9.5 %reduce-scatter.4.cloned.1.call-done = bf16[16,32,96]{2,1,0:T(8,128)(2,1)} async-done(((bf16[32,32,96]{2,1,0:T(8,128)(2,1)}), bf16[16,32,96]{2,1,0:T(8,128)(2,1)}) %reduce-scatter.4.cloned.1.call-update) | async-done | bytes 98320 | tf_op jit(solution)/shard_map/while/body/eval_jaxpr/reduce_scatter | solution.py:18
  302.9 21.7 %reduce-scatter.6.cloned.1.call-done = bf16[4,32,96]{2,1,0:T(8,128)(2,1)} async-done(((bf16[16,32,96]{2,1,0:T(8,128)(2,1)}), bf16[4,32,96]{2,1,0:T(8,128)(2,1)}) %reduce-scatter.6.cloned.1.call-update) | async-done | bytes 24592 | tf_op jit(solution)/shard_map/while/body/eval_jaxpr/reduce_scatter | solution.py:18
  324.7 22.3 %reduce-scatter.8.cloned.1.call-done = bf16[1,32,96]{2,1,0:T(8,128)(2,1)} async-done(((bf16[4,32,96]{2,1,0:T(8,128)(2,1)}), bf16[1,32,96]{2,1,0:T(8,128)(2,1)}) %reduce-scatter.8.cloned.1.call-update) | async-done | bytes 6160 | tf_op jit(solution)/shard_map/while/body/eval_jaxpr/reduce_scatter | solution.py:18
  347.0 0.7 bitcast_dynamic-update-slice_fusion.2
  347.7 3.1 collective-permute-start
  350.8 0.8 collective-permute-done
  351.6 0.7 stack.7
  352.3 9.3 %all-to-all-start = ((bf16[32,32,96]{2,1,0:T(8,128)(2,1)}), bf16[32,32,96]{2,1,0:T(8,128)(2,1)S(1)}, u32[]{:S(2)}, u32[]{:S(2)}) async-start(bf16[32,32,96]{2,1,0:T(8,128)(2,1)} %stack.7), calls=%async_computation | async-start | bytes 524288 | tf_op jit(solution)/shard_map/while/body/eval_jaxpr/all_to_all | solution.py:163
  361.7 8.8 %all-to-all-done = bf16[32,32,96]{2,1,0:T(8,128)(2,1)S(1)} async-done(((bf16[32,32,96]{2,1,0:T(8,128)(2,1)}), bf16[32,32,96]{2,1,0:T(8,128)(2,1)S(1)}, u32[]{:S(2)}, u32[]{:S(2)}) %all-to-all-start) | async-done | bytes 196640 | tf_op jit(solution)/shard_map/while/body/eval_jaxpr/all_to_all | solution.py:163
  371.8 0.8 reverse_reduce_fusion.2
  373.2 0.9 fusion.73
  374.4 0.7 copy.88
  375.2 9.5 %reduce-scatter.4.cloned.1.call-done = bf16[16,32,96]{2,1,0:T(8,128)(2,1)} async-done(((bf16[32,32,96]{2,1,0:T(8,128)(2,1)}), bf16[16,32,96]{2,1,0:T(8,128)(2,1)}) %reduce-scatter.4.cloned.1.call-update) | async-done | bytes 98320 | tf_op jit(solution)/shard_map/while/body/eval_jaxpr/reduce_scatter | solution.py:18
  384.8 21.6 %reduce-scatter.6.cloned.1.call-done = bf16[4,32,96]{2,1,0:T(8,128)(2,1)} async-done(((bf16[16,32,96]{2,1,0:T(8,128)(2,1)}), bf16[4,32,96]{2,1,0:T(8,128)(2,1)}) %reduce-scatter.6.cloned.1.call-update) | async-done | bytes 24592 | tf_op jit(solution)/shard_map/while/body/eval_jaxpr/reduce_scatter | solution.py:18
  406.4 22.3 %reduce-scatter.8.cloned.1.call-done = bf16[1,32,96]{2,1,0:T(8,128)(2,1)} async-done(((bf16[4,32,96]{2,1,0:T(8,128)(2,1)}), bf16[1,32,96]{2,1,0:T(8,128)(2,1)}) %reduce-scatter.8.cloned.1.call-update) | async-done | bytes 6160 | tf_op jit(solution)/shard_map/while/body/eval_jaxpr/reduce_scatter | solution.py:18
  429.4 3.1 collective-permute-start
  432.6 0.8 collective-permute-done
  433.3 10.0 %all-gather = bf16[8,32,96]{2,1,0:T(8,128)(2,1)S(1)} all-gather(bf16[2,32,96]{2,1,0:T(8,128)(2,1)S(1)} %get-tuple-element.349), channel_id=2, replica_groups=mesh['pp'=4,'fs'=4,'tp_0'=4,'tp_1'=2] {'pp'}, dimensions={0}, use_global_device_ids=true | all-gather | bytes 61440 | tf_op jit(solution)/shard_map/all_gather | solution.py:45
  443.5 42.5 %all-gather.2 = f32[32,2,24]{2,1,0:T(2,128)S(1)} all-gather(f32[1,2,24]{2,1,0:T(2,128)S(1)} %bitcast.184), channel_id=3, replica_groups=mesh['pp'=4,'fs'=4,'tp_0'=4,'tp_1'=2] {'tp_0','tp_1','fs'}, dimensions={0}, use_global_device_ids=true | all-gather | bytes 6336 | tf_op jit(solution)/shard_map/all_gather | solution.py:49
  (189 shorter events, 16.7 us)
Async XLA Ops:
  6.5 1.1 copy-start.3
  6.5 1.3 copy-start.10
  7.7 1.0 copy-start.1
  7.7 1.0 copy-start.2
  8.7 2.2 copy-start.9
  10.9 11.2 %copy-start = (bf16[1,1,1,64,1024]{4,3,2,1,0:T(8,128)(2,1)S(1)}, bf16[1,1,1,64,1024]{4,3,2,1,0:T(8,128)(2,1)}, u32[]{:S(2)}) copy-start(bf16[1,1,1,64,1024]{4,3,2,1,0:T(8,128)(2,1)} %param.29) | copy-start | bytes 393220
  21.3 0.8 copy-start.6
  21.3 0.8 copy-start.7
  21.4 0.7 copy-start.11
  22.0 0.7 copy-start.4
  22.1 0.7 copy-start.5
  22.1 0.7 copy-start.8
  23.5 20.5 %all-to-all-start = ((bf16[32,32,96]{2,1,0:T(8,128)(2,1)}), bf16[32,32,96]{2,1,0:T(8,128)(2,1)S(1)}, u32[]{:S(2)}, u32[]{:S(2)}) async-start(bf16[32,32,96]{2,1,0:T(8,128)(2,1)} %stack.7), calls=%async_computation | async-start | bytes 524288 | tf_op jit(solution)/shard_map/while/body/eval_jaxpr/all_to_all | solution.py:163
  35.2 21.7 %reduce-scatter.4.cloned.1.call-start = ((), (), s32[]{:S(2)}) async-start(), calls=%async_computation.4 | async-start | bytes 393216 | tf_op jit(solution)/shard_map/while/body/eval_jaxpr/reduce_scatter | solution.py:18
  48.7 29.9 %reduce-scatter.6.cloned.1.call-start = ((), (), s32[]{:S(2)}) async-start(), calls=%async_computation.5 | async-start | bytes 163840 | tf_op jit(solution)/shard_map/while/body/eval_jaxpr/reduce_scatter | solution.py:18
  56.9 44.3 %reduce-scatter.8.cloned.1.call-start = ((), (), s32[]{:S(2)}) async-start(), calls=%async_computation.6 | async-start | bytes 40960 | tf_op jit(solution)/shard_map/while/body/eval_jaxpr/reduce_scatter | solution.py:18
  101.9 3.9 collective-permute-start
  106.6 18.2 %all-to-all-start = ((bf16[32,32,96]{2,1,0:T(8,128)(2,1)}), bf16[32,32,96]{2,1,0:T(8,128)(2,1)S(1)}, u32[]{:S(2)}, u32[]{:S(2)}) async-start(bf16[32,32,96]{2,1,0:T(8,128)(2,1)} %stack.7), calls=%async_computation | async-start | bytes 524288 | tf_op jit(solution)/shard_map/while/body/eval_jaxpr/all_to_all | solution.py:163
  115.9 23.1 %reduce-scatter.4.cloned.1.call-start = ((), (), s32[]{:S(2)}) async-start(), calls=%async_computation.4 | async-start | bytes 393216 | tf_op jit(solution)/shard_map/while/body/eval_jaxpr/reduce_scatter | solution.py:18
  129.4 31.2 %reduce-scatter.6.cloned.1.call-start = ((), (), s32[]{:S(2)}) async-start(), calls=%async_computation.5 | async-start | bytes 163840 | tf_op jit(solution)/shard_map/while/body/eval_jaxpr/reduce_scatter | solution.py:18
  139.0 44.0 %reduce-scatter.8.cloned.1.call-start = ((), (), s32[]{:S(2)}) async-start(), calls=%async_computation.6 | async-start | bytes 40960 | tf_op jit(solution)/shard_map/while/body/eval_jaxpr/reduce_scatter | solution.py:18
  183.7 3.9 collective-permute-start
  188.3 18.2 %all-to-all-start = ((bf16[32,32,96]{2,1,0:T(8,128)(2,1)}), bf16[32,32,96]{2,1,0:T(8,128)(2,1)S(1)}, u32[]{:S(2)}, u32[]{:S(2)}) async-start(bf16[32,32,96]{2,1,0:T(8,128)(2,1)} %stack.7), calls=%async_computation | async-start | bytes 524288 | tf_op jit(solution)/shard_map/while/body/eval_jaxpr/all_to_all | solution.py:163
  197.6 23.1 %reduce-scatter.4.cloned.1.call-start = ((), (), s32[]{:S(2)}) async-start(), calls=%async_computation.4 | async-start | bytes 393216 | tf_op jit(solution)/shard_map/while/body/eval_jaxpr/reduce_scatter | solution.py:18
  211.2 31.4 %reduce-scatter.6.cloned.1.call-start = ((), (), s32[]{:S(2)}) async-start(), calls=%async_computation.5 | async-start | bytes 163840 | tf_op jit(solution)/shard_map/while/body/eval_jaxpr/reduce_scatter | solution.py:18
  220.7 44.3 %reduce-scatter.8.cloned.1.call-start = ((), (), s32[]{:S(2)}) async-start(), calls=%async_computation.6 | async-start | bytes 40960 | tf_op jit(solution)/shard_map/while/body/eval_jaxpr/reduce_scatter | solution.py:18
  265.8 3.9 collective-permute-start
  270.4 18.2 %all-to-all-start = ((bf16[32,32,96]{2,1,0:T(8,128)(2,1)}), bf16[32,32,96]{2,1,0:T(8,128)(2,1)S(1)}, u32[]{:S(2)}, u32[]{:S(2)}) async-start(bf16[32,32,96]{2,1,0:T(8,128)(2,1)} %stack.7), calls=%async_computation | async-start | bytes 524288 | tf_op jit(solution)/shard_map/while/body/eval_jaxpr/all_to_all | solution.py:163
  279.7 23.1 %reduce-scatter.4.cloned.1.call-start = ((), (), s32[]{:S(2)}) async-start(), calls=%async_computation.4 | async-start | bytes 393216 | tf_op jit(solution)/shard_map/while/body/eval_jaxpr/reduce_scatter | solution.py:18
  293.3 31.3 %reduce-scatter.6.cloned.1.call-start = ((), (), s32[]{:S(2)}) async-start(), calls=%async_computation.5 | async-start | bytes 163840 | tf_op jit(solution)/shard_map/while/body/eval_jaxpr/reduce_scatter | solution.py:18
  302.8 44.2 %reduce-scatter.8.cloned.1.call-start = ((), (), s32[]{:S(2)}) async-start(), calls=%async_computation.6 | async-start | bytes 40960 | tf_op jit(solution)/shard_map/while/body/eval_jaxpr/reduce_scatter | solution.py:18
  347.7 3.9 collective-permute-start
  352.3 18.2 %all-to-all-start = ((bf16[32,32,96]{2,1,0:T(8,128)(2,1)}), bf16[32,32,96]{2,1,0:T(8,128)(2,1)S(1)}, u32[]{:S(2)}, u32[]{:S(2)}) async-start(bf16[32,32,96]{2,1,0:T(8,128)(2,1)} %stack.7), calls=%async_computation | async-start | bytes 524288 | tf_op jit(solution)/shard_map/while/body/eval_jaxpr/all_to_all | solution.py:163
  361.6 23.1 %reduce-scatter.4.cloned.1.call-start = ((), (), s32[]{:S(2)}) async-start(), calls=%async_computation.4 | async-start | bytes 393216 | tf_op jit(solution)/shard_map/while/body/eval_jaxpr/reduce_scatter | solution.py:18
  375.2 31.2 %reduce-scatter.6.cloned.1.call-start = ((), (), s32[]{:S(2)}) async-start(), calls=%async_computation.5 | async-start | bytes 163840 | tf_op jit(solution)/shard_map/while/body/eval_jaxpr/reduce_scatter | solution.py:18
  384.7 44.0 %reduce-scatter.8.cloned.1.call-start = ((), (), s32[]{:S(2)}) async-start(), calls=%async_computation.6 | async-start | bytes 40960 | tf_op jit(solution)/shard_map/while/body/eval_jaxpr/reduce_scatter | solution.py:18
  429.4 3.9 collective-permute-start
Sparse Core Ops, SparseCore 0:
  48.8 7.9 reduce-scatter.3
  59.2 19.4 reduce-scatter.5
  81.0 20.1 reduce-scatter.7
  129.6 9.3 reduce-scatter.3
  141.2 19.4 reduce-scatter.5
  162.8 20.1 reduce-scatter.7
  211.3 9.3 reduce-scatter.3
  223.1 19.4 reduce-scatter.5
  244.9 20.1 reduce-scatter.7
  293.4 9.3 reduce-scatter.3
  305.1 19.4 reduce-scatter.5
  326.8 20.1 reduce-scatter.7
  375.3 9.3 reduce-scatter.3
  386.9 19.4 reduce-scatter.5
  408.6 20.1 reduce-scatter.7
